TPU v7x, 32 devices: a whole 2x2x4 slice. The times are simulated.
32 devices in a mesh: ep: 8 (over z, y), tp: 4 (over x, core).
Axes of the slice: x: 2, y: 2, z: 4, core: 2. Of those that a mesh axis runs over, the one named last changes fastest.
Arguments:
- queries: bfloat16 [4096, 1024], P('ep', 'tp'), may hold values from -6 to 6
- keys: bfloat16 [4096, 512], P('ep', 'tp'), may hold values from -6 to 6
- values: bfloat16 [4096, 512], P('ep', 'tp'), may hold values from -6 to 6
- forget_cache: float32 [8, 4096], P('tp'), may hold values from -412 to 0, as said below
- query_gain: float32 [128], replicated, may hold values from 0.6 to 6
- key_gain: float32 [128], replicated, may hold values from 0.6 to 6
- mixer_out: bfloat16 [1024, 2048], replicated, may hold values from -0.75 to 0.75
- expert_input: bfloat16 [4096, 2048], P(('ep', 'tp')), may hold values from -6 to 6
- norm_gain: float32 [2048], replicated, may hold values from 0.1 to 1.9
- routes: int32 [4096, 2], P(('ep', 'tp')), may hold values from 0 to 31, all different within a row; in each aligned block of 128 rows (0 to 127, 128 to 255, ...) at most 16 rows name the same one
- route_weights: float32 [4096, 2], P(('ep', 'tp')), may hold values from 0.1 to 1
- w_gate: bfloat16 [32, 2048, 1024], P('ep', None, 'tp'), may hold values from -0.125 to 0.125
- w_up: bfloat16 [32, 2048, 1024], P('ep', None, 'tp'), may hold values from -0.125 to 0.125
- w_down: bfloat16 [32, 2048, 1024], P('ep', None, 'tp'), may hold values from -0.1875 to 0.1875
Outputs:
- mixed: bfloat16 [4096, 2048], P(('ep', 'tp'))
- routed: bfloat16 [4096, 2048], P(('ep', 'tp'))
Inputs may be any that keep to these rules, and one draw needn't show every extreme that they name: `routes`: each row names 2 different experts; among the rows of one device no expert is named by more than 16 rows, a bound that some block reaches. `forget_cache`: never rises along the positions.
All inputs are finite; a program needn't handle non-finite values.
Results may differ from a plain program's by a relative error of at most 0.013.
The roundings to bfloat16 on the way count: a program that leaves them out, or rounds other values in their place, can miss the bound.
Values may be sent and summed in bfloat16 or wider, within the bound.
A program may use at most 128 MiB of HBM per device.

v0:
```python
import math
import jax
import jax.numpy as jnp
from jax import lax
from jax.sharding import PartitionSpec as P

EXPERTS = 32
CAP = 16
EPSILON = 1e-06
NEGATIVE = -1e30


def rms_scale(inputs, gain):
    inputs = inputs.astype(jnp.float32)
    return inputs * lax.rsqrt(jnp.mean(inputs * inputs, axis=-1, keepdims=True) + EPSILON) * gain


def attend(queries, keys, values, forget_cache, query_gain, key_gain):
    rows = queries.shape[0]
    head_dim = keys.shape[1]
    local_heads = forget_cache.shape[0]
    first = lax.axis_index("ep") * rows
    normed_q = rms_scale(queries.reshape(rows, local_heads, head_dim), query_gain).astype(
        jnp.bfloat16
    )
    normed_k = rms_scale(keys, key_gain).astype(jnp.bfloat16)
    scale = head_dim ** (-0.5)
    groups = [(normed_q, first + jnp.arange(rows, dtype=jnp.int32))]
    gate_sets = [jnp.take(forget_cache, position, axis=1) for _, position in groups]
    initial = tuple(
        (
            (
                jnp.full((local_heads, group_rows.shape[0]), NEGATIVE, jnp.float32),
                jnp.zeros((local_heads, group_rows.shape[0]), jnp.float32),
                jnp.zeros((local_heads, group_rows.shape[0], head_dim), jnp.float32),
            )
            for group_rows, _ in groups
        )
    )
    key_matrix_rows = lax.all_gather(normed_k, "ep", axis=0, tiled=True)
    value_rows = lax.all_gather(values, "ep", axis=0, tiled=True)
    length = key_matrix_rows.shape[0]
    width = math.gcd(length, 512)
    query_rows, query_pos = groups[0]
    query_gates = gate_sets[0]
    last_pos = jnp.max(query_pos)

    def one_block(number, inner):
        begin = number * width

        def update(current):
            highest, denom, accum = current
            block_keys = lax.dynamic_slice_in_dim(key_matrix_rows, number * width, width, 0)
            block_values = lax.dynamic_slice_in_dim(value_rows, number * width, width, 0)
            key_gates = lax.dynamic_slice_in_dim(forget_cache, begin, width, 1)
            scores = (
                jnp.einsum(
                    "qhd,kd->hqk", query_rows, block_keys, preferred_element_type=jnp.float32
                )
                * scale
            )
            scores = scores + query_gates[:, :, None] - key_gates[:, None, :]
            key_pos = begin + jnp.arange(width, dtype=jnp.int32)
            allowed = key_pos[None, :] <= query_pos[:, None]
            scores = jnp.where(allowed[None], scores, NEGATIVE)
            newest = jnp.maximum(highest, jnp.max(scores, axis=2))
            weights = jnp.where(allowed[None], jnp.exp(scores - newest[:, :, None]), 0.0)
            factor = jnp.exp(highest - newest)
            denom = denom * factor + jnp.sum(weights, axis=2)
            product = jnp.einsum(
                "hqk,kd->hqd",
                weights.astype(jnp.bfloat16),
                block_values,
                preferred_element_type=jnp.float32,
            )
            accum = accum * factor[:, :, None] + product
            return (newest, denom, accum)

        return lax.cond(begin <= last_pos, update, lambda current: current, inner)

    results = [lax.fori_loop(0, length // width, one_block, initial[0])]
    finals = tuple(results)
    outputs = [(accum / denom[:, :, None]).astype(jnp.bfloat16) for _, denom, accum in finals]
    return outputs[0]


def dispatch(expert_input, norm_gain, routes):
    rows = expert_input.shape[0]
    top = routes.shape[1]
    normed = rms_scale(expert_input, norm_gain).astype(jnp.bfloat16)
    flat = routes.reshape(-1)
    onehot = (flat[:, None] == jnp.arange(EXPERTS, dtype=jnp.int32)[None, :]).astype(jnp.int32)
    prior_state = jnp.cumsum(onehot, axis=0) - onehot
    rank = jnp.sum(prior_state * onehot, axis=1)
    slots = rank * EXPERTS + flat
    owner = (
        jnp.full((CAP * EXPERTS,), rows, jnp.int32)
        .at[slots]
        .set(jnp.arange(rows * top, dtype=jnp.int32) // top)
    )
    padded = jnp.concatenate([normed, jnp.zeros((1, normed.shape[1]), jnp.bfloat16)], axis=0)
    outgoing = padded[owner].reshape(CAP, EXPERTS, normed.shape[1])
    received = lax.all_to_all(outgoing, "ep", split_axis=1, concat_axis=0, tiled=True)
    return (received, slots)


def on_device(
    queries,
    keys,
    values,
    forget_cache,
    query_gain,
    key_gain,
    mixer_out,
    expert_input,
    norm_gain,
    routes,
    route_weights,
    w_gate,
    w_up,
    w_down,
):
    attended = attend(queries, keys, values, forget_cache, query_gain, key_gain)
    received, slots = dispatch(expert_input, norm_gain, routes)
    regrouped = lax.all_to_all(attended, "tp", split_axis=1, concat_axis=0, tiled=True)
    all_heads = regrouped.shape[0]
    projection = mixer_out.reshape(all_heads, regrouped.shape[2], mixer_out.shape[1])
    mixed = jnp.einsum(
        "hqd,hde->qe", regrouped, projection, preferred_element_type=jnp.float32
    ).astype(jnp.bfloat16)
    pieces = lax.all_gather(received, "tp", axis=0, tiled=True)
    gate = jnp.einsum("red,edf->ref", pieces, w_gate, preferred_element_type=jnp.float32)
    upward = jnp.einsum("red,edf->ref", pieces, w_up, preferred_element_type=jnp.float32)
    hidden = (jax.nn.silu(gate) * upward).astype(jnp.bfloat16)
    summed = lax.psum_scatter(
        jnp.einsum("ref,edf->red", hidden, w_down, preferred_element_type=jnp.float32).astype(
            jnp.bfloat16
        ),
        "tp",
        scatter_dimension=0,
        tiled=True,
    )
    returned = lax.all_to_all(summed, "ep", split_axis=0, concat_axis=1, tiled=True)
    flat_back = returned.reshape(-1, returned.shape[2])
    picked = (
        flat_back[slots]
        .reshape(routes.shape[0], routes.shape[1], returned.shape[2])
        .astype(jnp.float32)
    )
    routed = jnp.sum(picked * route_weights[:, :, None], axis=1).astype(jnp.bfloat16)
    return (mixed, routed)


def solution(mesh):
    in_specs = (
        P("ep", "tp"),
        P("ep", "tp"),
        P("ep", "tp"),
        P("tp", None),
        P(),
        P(),
        P(),
        P(("ep", "tp"), None),
        P(),
        P(("ep", "tp"), None),
        P(("ep", "tp"), None),
        P("ep", None, "tp"),
        P("ep", None, "tp"),
        P("ep", None, "tp"),
    )
    out_specs = (P(("ep", "tp"), None), P(("ep", "tp"), None))
    return jax.shard_map(
        on_device, mesh=mesh, in_specs=in_specs, out_specs=out_specs, check_vma=False
    )
```

profile of v0, /device:TPU:0, one launch (start us, length us, event | category | flops | bytes accessed | tf_op | source)
XLA Modules:
  0.0 367.3 jit_solution(14982361686460898123)
XLA Ops:
  7.2 0.8 copy.60
  8.1 0.1 eq.25
  8.3 0.1 reshape.154
  8.4 0.6 reduce-window.6
  9.0 0.2 slice_reduce_fusion
  9.4 1.4 scatter_custom_fusion
  10.8 1.2 fusion.22
  12.1 1.2 fusion.24
  13.4 2.5 gather_fusion.1
  15.8 1.2 copy.64
  17.0 55.3 %all_to_all.51 = bf16[16,32,2048]{2,0,1:T(8,128)(2,1)S(1)} all-to-all(bf16[16,32,2048]{2,0,1:T(8,128)(2,1)S(1)} %copy.64), channel_id=1, replica_groups=mesh['ep'=8,'tp'=4] {'ep'}, dimensions={1} | all-to-all | bytes 4194304 | tf_op jit(solution)/shard_map/all_to_all | solution.py:103
  72.3 1.5 copy.65
  73.9 0.8 copy-done
  74.7 0.1 fusion.28
  74.9 0.8 fusion.30
  75.8 0.7 all-gather.6.cloned.1.call-update
  76.5 0.2 reduce-scatter.2.cloned.1.call-start
  76.7 54.6 %all-gather.8.cloned.1.call-done = bf16[512,4,2048]{2,0,1:T(8,128)(2,1)} async-done(((bf16[128,4,2048]{2,0,1:T(8,128)(2,1)}), bf16[512,4,2048]{2,0,1:T(8,128)(2,1)}) %all-gather.8.cloned.1.call-update) | async-done | bytes 8388624 | tf_op jit(solution)/shard_map/all_gather | solution.py:131
  131.3 6.9 %fusion.42 = f32[4,512,256]{2,1,0:T(8,128)S(1)} fusion(bf16[512,4,2048]{2,0,1:T(8,128)(2,1)} %all-gather.8.cloned.1.call-done, bf16[4,2048,256]{2,1,0:T(8,128)(2,1)} %param.29), kind=kOutput, calls=%fused_computation.89 | convolution fusion | flops 2147483648 | bytes 14680064 | tf_op jit(solution)/shard_map/red,edf->ref/dot_general | solution.py:132
  138.2 14.0 %convert_bitcast_fusion = bf16[512,4,2048]{2,0,1:T(8,128)(2,1)} fusion(bf16[4,2048,256]{2,1,0:T(8,128)(2,1)} %param.31, f32[4,512,256]{2,1,0:T(8,128)S(1)} %fusion.42, bf16[512,4,2048]{2,0,1:T(8,128)(2,1)} %all-gather.8.cloned.1.call-done, bf16[4,2048,256]{2,1,0:T(8,128)(2,1)} %param.30), kind=kOutput, calls=%fused_computation.28 | convolution fusion | flops 4302307328 | bytes 27262976 | tf_op jit(solution)/shard_map/ref,edf->red/dot_general | solution.py:136
  152.2 0.7 copy-done.2
  153.0 0.7 copy.55
  153.6 0.6 fusion.35
  154.2 1.0 gather_fusion
  155.3 0.1 select_bitcast_fusion
  155.5 0.2 copy.54
  155.9 0.2 copy.56
  156.1 18.2 %all-gather.4.cloned.1.call-done = bf16[4096,128]{1,0:T(8,128)(2,1)} async-done(((bf16[512,128]{1,0:T(8,128)(2,1)}), bf16[4096,128]{1,0:T(8,128)(2,1)}) %all-gather.4.cloned.1.call-update) | async-done | bytes 1048592 | tf_op jit(solution)/shard_map/all_gather | solution.py:40
  174.3 41.2 %all-gather.6.cloned.1.call-done = bf16[4096,128]{1,0:T(8,128)(2,1)} async-done(((bf16[512,128]{1,0:T(8,128)(2,1)}), bf16[4096,128]{1,0:T(8,128)(2,1)}) %all-gather.6.cloned.1.call-update) | async-done | bytes 1048592 | tf_op jit(solution)/shard_map/all_gather | solution.py:41
  215.5 8.8 %while.18 = (s32[]{:T(128)}, f32[2,512]{1,0:T(2,128)S(1)}, f32[2,512]{1,0:T(2,128)S(1)}, f32[2,512,128]{2,1,0:T(8,128)S(1)}, s32[]{:T(128)}, /*index=5*/bf16[409...) while((s32[]{:T(128)}, f32[2,512]{1,0:T(2,128)S(1)}, ...), condition=%wide.region_8.9_spmd.clone, body=%wide.region_3.8_spmd.clone.sunk | while | flops 274729984 | bytes 9007507 | solution.py:81
  216.1 4.0 %conditional.3 = ((f32[2,512]{1,0:T(2,128)S(1)}, f32[2,512]{1,0:T(2,128)S(1)}, f32[2,512,128]{2,1,0:T(8,128)S(1)})) conditional(s32[]{:T(128)} %convert_element_type.114, (f32[2,512]{1,0:T(2,128)S(1)}, f32[2,512]{1,0:T(2,128)S(1)}, f32[2,512,128]{2,1,0:T(8,128)S(1)}) %tuple.53, (s32[]{:T(128)}, s32[]{:T(128)}, s32[]{:T(128)}, ...), branch_computations={%region_4.4_spmd, %region_5.0_spmd} | conditional | flops 274729984 | bytes 9005188 | solution.py:79
  216.1 0.2 broadcast_compare_fusion
  216.4 1.6 fusion.41
  218.0 0.4 fusion.5
  218.4 1.7 convolution_add_fusion
  224.3 0.2 divide_convert_fusion
  224.5 1.0 copy.58
  225.5 3.6 all-to-all-start
  229.1 58.9 %reduce-scatter.2.cloned.1.call-done = bf16[128,4,2048]{2,0,1:T(8,128)(2,1)} async-done(((bf16[512,4,2048]{2,0,1:T(8,128)(2,1)}), bf16[128,4,2048]{2,0,1:T(8,128)(2,1)}) %reduce-scatter.2.cloned.1.call-update) | async-done | bytes 2097168 | tf_op jit(solution)/shard_map/reduce_scatter | solution.py:135
  288.0 4.6 %copy.66 = bf16[128,4,2048]{2,1,0:T(4,128)(2,1)} copy(bf16[128,4,2048]{2,0,1:T(8,128)(2,1)} %reduce-scatter.2.cloned.1.call-done) | data formatting | bytes 4194304 | tf_op jit(solution)/shard_map/reduce_scatter | solution.py:135
  292.6 8.5 %all-to-all-start.2 = ((bf16[128,4,2048]{2,1,0:T(4,128)(2,1)}), bf16[128,4,2048]{2,1,0:T(4,128)(2,1)S(1)}, u32[]{:S(2)}, u32[]{:S(2)}) async-start(bf16[128,4,2048]{2,1,0:T(4,128)(2,1)} %copy.66), calls=%async_computation.3 | async-start | bytes 4194304 | tf_op jit(solution)/shard_map/all_to_all | solution.py:143
  301.2 3.7 %fusion.17 = bf16[128,2048]{1,0:T(8,128)(2,1)} fusion(bf16[8,128,128]{2,1,0:T(8,128)(2,1)S(1)} %bitcast.110, bf16[8,128,2048]{2,1,0:T(8,128)(2,1)} %bitcast.109), kind=kOutput, calls=%fused_computation.30 | convolution fusion | flops 537133056 | bytes 4980736 | tf_op jit(solution)/shard_map/hqd,hde->qe/dot_general | solution.py:128
  304.9 44.2 %all-to-all-done.2 = bf16[128,4,2048]{2,1,0:T(4,128)(2,1)S(1)} async-done(((bf16[128,4,2048]{2,1,0:T(4,128)(2,1)}), bf16[128,4,2048]{2,1,0:T(4,128)(2,1)S(1)}, u32[]{:S(2)}, u32[]{:S(2)}) %all-to-all-start.2) | async-done | bytes 2097184 | tf_op jit(solution)/shard_map/all_to_all | solution.py:143
  349.1 2.4 copy.73
  351.5 2.5 reshape.156
  354.0 1.4 gather_fusion.2
  355.4 1.3 reshape.158
  356.7 4.0 %multiply_reduce_fusion = bf16[128,2048]{1,0:T(8,128)(2,1)} fusion(f32[128,2,2048]{2,1,0:T(2,128)S(1)} %reshape.158, f32[128,2]{1,0:T(8,128)S(1)} %copy.68), kind=kLoop, calls=%fused_computation.39 | loop fusion | flops 786432 | bytes 2622464 | tf_op jit(solution)/shard_map/reduce_sum | solution.py:150
  (63 shorter events, 1.2 us)
Async XLA Ops:
  7.2 124.1 %all-gather.8.cloned.1.call-start = ((), (), s32[]{:S(2)}) async-start(), calls=%async_computation.6 | async-start | bytes 10485760 | tf_op jit(solution)/shard_map/all_gather | solution.py:131
  73.8 0.9 copy-start
  73.8 1.1 copy-start.4
  73.8 100.4 %all-gather.4.cloned.1.call-start = ((), (), s32[]{:S(2)}) async-start(), calls=%async_computation.4 | async-start | bytes 1179648 | tf_op jit(solution)/shard_map/all_gather | solution.py:40
  75.7 139.7 %all-gather.6.cloned.1.call-start = ((), (), s32[]{:S(2)}) async-start(), calls=%async_computation.5 | async-start | bytes 1179648 | tf_op jit(solution)/shard_map/all_gather | solution.py:41
  76.5 211.6 %reduce-scatter.2.cloned.1.call-start = ((), (), s32[]{:S(2)}) async-start(), calls=%async_computation.7 | async-start | bytes 10485760 | tf_op jit(solution)/shard_map/reduce_scatter | solution.py:135
  152.2 0.8 copy-start.2
  152.2 3.3 copy-start.1
  152.2 3.6 copy-start.5
  225.5 67.1 %all-to-all-start = ((bf16[2,512,128]{2,0,1:T(2,128)(2,1)}), bf16[2,512,128]{2,0,1:T(2,128)(2,1)S(1)}, u32[]{:S(2)}, u32[]{:S(2)}) async-start(bf16[2,512,128]{2,0,1:T(2,128)(2,1)} %copy.58), calls=%async_computation | async-start | bytes 524288 | tf_op jit(solution)/shard_map/all_to_all | solution.py:125
  292.6 8.5 %copy-start.3 = (f32[128,2]{0,1:T(2,128)S(1)}, f32[128,2]{0,1:T(2,128)}, u32[]{:S(2)}) copy-start(f32[128,2]{0,1:T(2,128)} %param.28) | copy-start | bytes 3076
  292.6 56.5 %all-to-all-start.2 = ((bf16[128,4,2048]{2,1,0:T(4,128)(2,1)}), bf16[128,4,2048]{2,1,0:T(4,128)(2,1)S(1)}, u32[]{:S(2)}, u32[]{:S(2)}) async-start(bf16[128,4,2048]{2,1,0:T(4,128)(2,1)} %copy.66), calls=%async_computation.3 | async-start | bytes 4194304 | tf_op jit(solution)/shard_map/all_to_all | solution.py:143
Sparse Core Ops, SparseCore 0:
  74.0 57.2 all-gather.7
  134.0 40.2 all-gather.3
  176.4 38.9 all-gather.5
  217.9 70.0 reduce-scatter.1
where the time goes:
time: 368 us; the launch traced here: 367 us
  waiting for transfers between devices  218 us (59%)
  blocking collectives  55.3 us (15%)
  matrix products  27.9 us (8%)
  local copies, waits for them, and re-layouts  25 us (7%)
  between operations  14 us (4%)
  starting transfers between devices  12.5 us (3%)
  other arithmetic  10.1 us (3%)
  loops' own time  4.82 us (1%)
    reduce_scatter x1, waiting for transfers between devices, on_device(): lax.psum_scatter(jnp.einsum('ref,edf->red', hidden, w_down, preferred_ele...  58.9 us
    all_to_all x1, blocking collectives, dispatch(): lax.all_to_all(outgoing, 'ep', split_axis=1, concat_axis=0, tiled=True)  55.3 us
    all_gather x1, waiting for transfers between devices, on_device(): pieces = lax.all_gather(received, 'tp', axis=0, tiled=True)  54.6 us
    all_to_all x1, waiting for transfers between devices, on_device(): lax.all_to_all(summed, 'ep', split_axis=0, concat_axis=1, tiled=True)  44.2 us
    all_gather x1, waiting for transfers between devices, attend(): value_rows = lax.all_gather(values, 'ep', axis=0, tiled=True)  41.2 us
    all_gather x1, waiting for transfers between devices, attend(): key_matrix_rows = lax.all_gather(normed_k, 'ep', axis=0, tiled=True)  18.2 us
    dot_general x1, matrix products, on_device(): jnp.einsum('ref,edf->red', hidden, w_down, preferred_element_type=jnp.flo...  14 us
    all_to_all x1, starting transfers between devices, on_device(): lax.all_to_all(summed, 'ep', split_axis=0, concat_axis=1, tiled=True)  8.48 us
  transfers between devices with their start and end apart: 6, of which 5 were waited for; matrix products, arithmetic and copies ran while one was open for 10% of the time, Pallas kernels for 0%

commit v1 on v0

--- a/solution.py
+++ b/solution.py
@@ -8,6 +8,17 @@
 CAP = 16
 EPSILON = 1e-06
 NEGATIVE = -1e30
+
+
+def pass_along(x, mesh_axis, d):
+    peers = lax.axis_size(mesh_axis)
+    right = [(i, (i + 1) % peers) for i in range(peers)]
+    pieces = [x]
+    for far in range(1, peers):
+        pieces = [lax.ppermute(pieces[0], mesh_axis, right), *pieces]
+    whole = jnp.concatenate(pieces, axis=d)
+    shift = (lax.axis_index(mesh_axis) + 1) * pieces[-1].shape[d]
+    return jnp.roll(whole, shift, axis=d)
 
 
 def rms_scale(inputs, gain):
@@ -128,7 +139,7 @@
     mixed = jnp.einsum(
         "hqd,hde->qe", regrouped, projection, preferred_element_type=jnp.float32
     ).astype(jnp.bfloat16)
-    pieces = lax.all_gather(received, "tp", axis=0, tiled=True)
+    pieces = pass_along(received, "tp", 0)
     gate = jnp.einsum("red,edf->ref", pieces, w_gate, preferred_element_type=jnp.float32)
     upward = jnp.einsum("red,edf->ref", pieces, w_up, preferred_element_type=jnp.float32)
     hidden = (jax.nn.silu(gate) * upward).astype(jnp.bfloat16)

time: 368 us -> 335 us (0.910)
  waiting for transfers between devices: 218 us -> 175 us
  local copies, waits for them, and re-layouts: 25 us -> 38.4 us
  starting transfers between devices: 12.5 us -> 8.74 us
    ppermute x0 -> x3, waiting for transfers between devices: none -> 74.8 us  [pass_along(): pieces = [lax.ppermute(pieces[0], mesh_axis, right), *pieces]]
    all_gather x1 -> x0, waiting for transfers between devices: 54.6 us -> none  [on_device(): pieces = lax.all_gather(received, 'tp', axis=0, tiled=True)]
    reduce_scatter x1, waiting for transfers between devices: 58.9 us -> 35.3 us  [on_device(): lax.psum_scatter(jnp.einsum('ref,edf->red', hidden, w_down, preferred_ele...]
    all_gather x1, waiting for transfers between devices: 41.2 us -> 19.6 us  [attend(): value_rows = lax.all_gather(values, 'ep', axis=0, tiled=True)]
    all_gather x1, waiting for transfers between devices: 18.2 us -> 0.02 us  [attend(): key_matrix_rows = lax.all_gather(normed_k, 'ep', axis=0, tiled=True)]
    unnamed x18 -> x31, local copies, waits for them, and re-layouts: 3.55 us -> 17.8 us
    all_to_all x1, starting transfers between devices: 8.48 us -> 4.74 us  [on_device(): lax.all_to_all(summed, 'ep', split_axis=0, concat_axis=1, tiled=True)]
  transfers between devices with their start and end apart: 6 -> 8, of which waited for: 5 -> 6; matrix products, arithmetic and copies ran while one was open for 10% -> 13% of each run, Pallas kernels for 0% -> 0%
where the time goes in v1:
time: 335 us; the launch traced here: 334 us
  waiting for transfers between devices  175 us (52%)
  blocking collectives  55.3 us (17%)
  local copies, waits for them, and re-layouts  38.4 us (11%)
  matrix products  25.4 us (8%)
  between operations  15.9 us (5%)
  other arithmetic  10 us (3%)
  starting transfers between devices  8.74 us (3%)
  loops' own time  5.28 us (2%)
    ppermute x3, waiting for transfers between devices, pass_along(): pieces = [lax.ppermute(pieces[0], mesh_axis, right), *pieces]  74.8 us
    all_to_all x1, blocking collectives, dispatch(): lax.all_to_all(outgoing, 'ep', split_axis=1, concat_axis=0, tiled=True)  55.3 us
    all_to_all x1, waiting for transfers between devices, on_device(): lax.all_to_all(summed, 'ep', split_axis=0, concat_axis=1, tiled=True)  44.1 us
    reduce_scatter x1, waiting for transfers between devices, on_device(): lax.psum_scatter(jnp.einsum('ref,edf->red', hidden, w_down, preferred_ele...  35.3 us
    all_gather x1, waiting for transfers between devices, attend(): value_rows = lax.all_gather(values, 'ep', axis=0, tiled=True)  19.6 us
    unnamed x31, local copies, waits for them, and re-layouts  17.8 us
    dot_general x1, matrix products, on_device(): jnp.einsum('ref,edf->red', hidden, w_down, preferred_element_type=jnp.flo...  13.8 us
  transfers between devices with their start and end apart: 8, of which 6 were waited for; matrix products, arithmetic and copies ran while one was open for 13% of the time, Pallas kernels for 0%

profile of v1, /device:TPU:0, one launch (start us, length us, event | category | flops | bytes accessed | tf_op | source)
XLA Modules:
  0.0 333.6 jit_solution(10587660526966371674)
XLA Ops:
  8.0 0.8 copy.60
  9.3 0.6 reduce-window.6
  9.9 0.2 slice_reduce_fusion
  10.2 1.4 scatter_custom_fusion
  11.7 1.2 fusion.28
  12.9 1.2 fusion.30
  14.2 2.5 gather_fusion.1
  16.7 1.2 copy.64
  17.8 55.3 %all_to_all.51 = bf16[16,32,2048]{2,0,1:T(8,128)(2,1)S(1)} all-to-all(bf16[16,32,2048]{2,0,1:T(8,128)(2,1)S(1)} %copy.64), channel_id=1, replica_groups=mesh['ep'=8,'tp'=4] {'ep'}, dimensions={1} | all-to-all | bytes 4194304 | tf_op jit(solution)/shard_map/all_to_all | solution.py:114
  73.4 25.4 %collective-permute-done = bf16[128,4,2048]{2,0,1:T(8,128)(2,1)S(1)} collective-permute-done((bf16[128,4,2048]{2,0,1:T(8,128)(2,1)S(1)}, bf16[128,4,2048]{2,0,1:T(8,128)(2,1)S(1)}, u32[]{:S(2)}, u32[]{:S(2)}) %collective-permute-start) | collective-permute-done | bytes 2097184 | tf_op jit(solution)/shard_map/ppermute | solution.py:18
  98.8 1.3 copy-done
  100.3 25.4 %collective-permute-done.1 = bf16[128,4,2048]{2,0,1:T(8,128)(2,1)} collective-permute-done((bf16[128,4,2048]{2,0,1:T(8,128)(2,1)S(1)}, bf16[128,4,2048]{2,0,1:T(8,128)(2,1)}, u32[]{:S(2)}, u32[]{:S(2)}) %collective-permute-start.1) | collective-permute-done | bytes 2097184 | tf_op jit(solution)/shard_map/ppermute | solution.py:18
  125.7 0.8 fusion.38
  126.6 0.7 all-gather.5.cloned.1.call-update
  127.3 0.2 reduce-scatter.2.cloned.1.call-start
  127.5 23.9 %collective-permute-done.2 = bf16[128,4,2048]{2,0,1:T(8,128)(2,1)} collective-permute-done((bf16[128,4,2048]{2,0,1:T(8,128)(2,1)}, bf16[128,4,2048]{2,0,1:T(8,128)(2,1)}, u32[]{:S(2)}, u32[]{:S(2)}) %collective-permute-start.2) | collective-permute-done | bytes 2097184 | tf_op jit(solution)/shard_map/ppermute | solution.py:18
  151.5 1.8 constant_dynamic-update-slice_fusion.7
  153.3 2.0 constant_dynamic-update-slice_fusion.6
  155.3 0.2 copy-done.1
  155.8 1.8 constant_dynamic-update-slice_fusion.3
  157.6 1.8 constant_dynamic-update-slice_fusion.2
  159.8 5.7 %copy-done.3 = bf16[1024,4,2048]{2,0,1:T(8,128)(2,1)} copy-done((bf16[1024,4,2048]{2,0,1:T(8,128)(2,1)}, bf16[1024,4,2048]{2,0,1:T(8,128)(2,1)S(1)}, u32[]{:S(2)}) %copy-start.3) | copy-done | bytes 16777240
  165.5 4.5 %fusion.19 = f32[4,512,256]{2,1,0:T(8,128)S(1)} fusion(bf16[4,2048,256]{2,1,0:T(8,128)(2,1)} %param.29, bf16[1024,4,2048]{2,0,1:T(8,128)(2,1)S(1)} %constant_dynamic-update-slice_fusion, s32[]{:T(128)S(6)} %select_n.73), kind=kOutput, calls=%fused_computation.31 | convolution fusion | flops 2147483648 | bytes 14680068 | tf_op jit(solution)/shard_map/red,edf->ref/dot_general | solution.py:143
  170.1 13.8 %convert_bitcast_fusion = bf16[512,4,2048]{2,0,1:T(8,128)(2,1)} fusion(bf16[4,2048,256]{2,1,0:T(8,128)(2,1)} %param.31, f32[4,512,256]{2,1,0:T(8,128)S(1)} %fusion.19, bf16[4,2048,256]{2,1,0:T(8,128)(2,1)} %param.30, bf16[1024,4,2048]{2,0,1:T(8,128)(2,1)} %copy-done.3, s32[]{:T(128)S(6)} %select_n.73), kind=kOutput, calls=%fused_computation.28 | convolution fusion | flops 4302307328 | bytes 27262980 | tf_op jit(solution)/shard_map/ref,edf->red/dot_general | solution.py:147
  183.9 0.7 copy-done.5
  184.6 0.6 copy.55
  185.2 0.7 fusion.43
  185.9 1.0 gather_fusion
  187.8 19.6 %all-gather.5.cloned.1.call-done = bf16[4096,128]{1,0:T(8,128)(2,1)} async-done(((bf16[512,128]{1,0:T(8,128)(2,1)}), bf16[4096,128]{1,0:T(8,128)(2,1)}) %all-gather.5.cloned.1.call-update) | async-done | bytes 1048592 | tf_op jit(solution)/shard_map/all_gather | solution.py:52
  207.5 9.3 %while.18 = (s32[]{:T(128)}, f32[2,512]{1,0:T(2,128)S(1)}, f32[2,512]{1,0:T(2,128)S(1)}, f32[2,512,128]{2,1,0:T(8,128)S(1)}, s32[]{:T(128)}, /*index=5*/bf16[409...) while((s32[]{:T(128)}, f32[2,512]{1,0:T(2,128)S(1)}, ...), condition=%wide.region_8.9_spmd.clone, body=%wide.region_3.8_spmd.clone.sunk | while | flops 274729984 | bytes 9007507 | solution.py:92
  208.1 4.1 %conditional.3 = ((f32[2,512]{1,0:T(2,128)S(1)}, f32[2,512]{1,0:T(2,128)S(1)}, f32[2,512,128]{2,1,0:T(8,128)S(1)})) conditional(s32[]{:T(128)} %convert_element_type.112, (f32[2,512]{1,0:T(2,128)S(1)}, f32[2,512]{1,0:T(2,128)S(1)}, f32[2,512,128]{2,1,0:T(8,128)S(1)}) %tuple.54, (s32[]{:T(128)}, s32[]{:T(128)}, s32[]{:T(128)}, ...), branch_computations={%region_4.4_spmd, %region_5.0_spmd} | conditional | flops 274729984 | bytes 9005188 | solution.py:90
  208.2 0.2 broadcast_compare_fusion
  208.4 1.6 fusion.53
  210.1 0.4 fusion.5
  210.5 1.7 convolution_add_fusion
  216.8 0.2 divide_convert_fusion
  217.0 1.0 copy.58
  218.0 3.6 %all-to-all-start = ((bf16[2,512,128]{2,0,1:T(2,128)(2,1)}), bf16[2,512,128]{2,0,1:T(2,128)(2,1)S(1)}, u32[]{:S(2)}, u32[]{:S(2)}) async-start(bf16[2,512,128]{2,0,1:T(2,128)(2,1)} %copy.58), calls=%async_computation | async-start | bytes 524288 | tf_op jit(solution)/shard_map/all_to_all | solution.py:136
  221.6 35.3 %reduce-scatter.2.cloned.1.call-done = bf16[128,4,2048]{2,0,1:T(8,128)(2,1)} async-done(((bf16[512,4,2048]{2,0,1:T(8,128)(2,1)}), bf16[128,4,2048]{2,0,1:T(8,128)(2,1)}) %reduce-scatter.2.cloned.1.call-update) | async-done | bytes 2097168 | tf_op jit(solution)/shard_map/reduce_scatter | solution.py:146
  256.9 4.5 %copy.66 = bf16[128,4,2048]{2,1,0:T(4,128)(2,1)} copy(bf16[128,4,2048]{2,0,1:T(8,128)(2,1)} %reduce-scatter.2.cloned.1.call-done) | data formatting | bytes 4194304 | tf_op jit(solution)/shard_map/reduce_scatter | solution.py:146
  261.4 4.7 %all-to-all-start.2 = ((bf16[128,4,2048]{2,1,0:T(4,128)(2,1)}), bf16[128,4,2048]{2,1,0:T(4,128)(2,1)S(1)}, u32[]{:S(2)}, u32[]{:S(2)}) async-start(bf16[128,4,2048]{2,1,0:T(4,128)(2,1)} %copy.66), calls=%async_computation.3 | async-start | bytes 4194304 | tf_op jit(solution)/shard_map/all_to_all | solution.py:154
  266.3 3.7 %fusion.21 = bf16[128,2048]{1,0:T(8,128)(2,1)} fusion(bf16[8,128,128]{2,1,0:T(8,128)(2,1)S(1)} %bitcast.97, bf16[8,128,2048]{2,1,0:T(8,128)(2,1)} %bitcast.96), kind=kOutput, calls=%fused_computation.34 | convolution fusion | flops 537133056 | bytes 4980736 | tf_op jit(solution)/shard_map/hqd,hde->qe/dot_general | solution.py:139
  270.1 44.1 %all-to-all-done.2 = bf16[128,4,2048]{2,1,0:T(4,128)(2,1)S(1)} async-done(((bf16[128,4,2048]{2,1,0:T(4,128)(2,1)}), bf16[128,4,2048]{2,1,0:T(4,128)(2,1)S(1)}, u32[]{:S(2)}, u32[]{:S(2)}) %all-to-all-start.2) | async-done | bytes 2097184 | tf_op jit(solution)/shard_map/all_to_all | solution.py:154
  314.2 2.7 copy.73
  316.9 2.5 reshape.156
  319.5 1.4 gather_fusion.2
  320.9 1.3 reshape.158
  322.2 3.9 %multiply_reduce_fusion = bf16[128,2048]{1,0:T(8,128)(2,1)} fusion(f32[128,2,2048]{2,1,0:T(2,128)S(1)} %reshape.158, f32[128,2]{1,0:T(8,128)S(1)} %copy.68), kind=kLoop, calls=%fused_computation.43 | loop fusion | flops 786432 | bytes 2622464 | tf_op jit(solution)/shard_map/reduce_sum | solution.py:161
  (79 shorter events, 2.8 us)
Async XLA Ops:
  8.0 179.8 %all-gather.3.cloned.1.call-start = ((), (), s32[]{:S(2)}) async-start(), calls=%async_computation.4 | async-start | bytes 1179648 | tf_op jit(solution)/shard_map/all_gather | solution.py:51
  73.2 27.0 %copy-start.2 = (bf16[512,128]{1,0:T(8,128)(2,1)S(1)}, bf16[512,128]{1,0:T(8,128)(2,1)}, u32[]{:S(2)}) copy-start(bf16[512,128]{1,0:T(8,128)(2,1)} %param.19) | copy-start | bytes 393220
  73.2 52.5 %copy-start.7 = (f32[128]{0:T(128)S(1)}, f32[128]{0:T(128)}, u32[]{:S(2)}) copy-start(f32[128]{0:T(128)} %param.23) | copy-start | bytes 1540
  73.3 25.5 %collective-permute-start = (bf16[128,4,2048]{2,0,1:T(8,128)(2,1)S(1)}, bf16[128,4,2048]{2,0,1:T(8,128)(2,1)S(1)}, u32[]{:S(2)}, u32[]{:S(2)}) collective-permute-start(bf16[128,4,2048]{2,0,1:T(8,128)(2,1)S(1)} %bitcast.89), channel_id=1, source_target_pairs={{0,1},{1,2},{2,3},{3,0},{4,5},{5,6},{6,7},{7,4},{8,9},{9,10},{10,1... | collective-permute-start | bytes 6291464 | tf_op jit(solution)/shard_map/ppermute | solution.py:18
  98.8 1.3 copy-start
  100.1 25.6 %collective-permute-start.1 = (bf16[128,4,2048]{2,0,1:T(8,128)(2,1)S(1)}, bf16[128,4,2048]{2,0,1:T(8,128)(2,1)}, u32[]{:S(2)}, u32[]{:S(2)}) collective-permute-start(bf16[128,4,2048]{2,0,1:T(8,128)(2,1)S(1)} %collective-permute-done), channel_id=1, source_target_pairs={{0,1},{1,2},{2,3},{3,0},{4,5},{5,6},{6,7},{7,4},{8,9},{9,10},{10,1... | collective-permute-start | bytes 6291464 | tf_op jit(solution)/shard_map/ppermute | solution.py:18
  125.7 25.8 %collective-permute-start.2 = (bf16[128,4,2048]{2,0,1:T(8,128)(2,1)}, bf16[128,4,2048]{2,0,1:T(8,128)(2,1)}, u32[]{:S(2)}, u32[]{:S(2)}) collective-permute-start(bf16[128,4,2048]{2,0,1:T(8,128)(2,1)} %collective-permute-done.1), channel_id=1, source_target_pairs={{0,1},{1,2},{2,3},{3,0},{4,5},{5,6},{6,7},{7,4},{8,9},{9,10},{10,1... | collective-permute-start | bytes 6291464 | tf_op jit(solution)/shard_map/ppermute | solution.py:18
  126.5 80.9 %all-gather.5.cloned.1.call-start = ((), (), s32[]{:S(2)}) async-start(), calls=%async_computation.5 | async-start | bytes 1179648 | tf_op jit(solution)/shard_map/all_gather | solution.py:52
  127.3 129.7 %reduce-scatter.2.cloned.1.call-start = ((), (), s32[]{:S(2)}) async-start(), calls=%async_computation.6 | async-start | bytes 10485760 | tf_op jit(solution)/shard_map/reduce_scatter | solution.py:146
  153.3 2.2 copy-start.1
  159.8 5.7 %copy-start.3 = (bf16[1024,4,2048]{2,0,1:T(8,128)(2,1)}, bf16[1024,4,2048]{2,0,1:T(8,128)(2,1)S(1)}, u32[]{:S(2)}) copy-start(bf16[1024,4,2048]{2,0,1:T(8,128)(2,1)S(1)} %constant_dynamic-update-slice_fusion) | copy-start | bytes 50331652
  183.8 0.8 copy-start.5
  183.9 3.4 %copy-start.4 = (bf16[512,256]{1,0:T(8,128)(2,1)S(1)}, bf16[512,256]{1,0:T(8,128)(2,1)}, u32[]{:S(2)}) copy-start(bf16[512,256]{1,0:T(8,128)(2,1)} %param.18) | copy-start | bytes 786436
  183.9 3.6 %copy-start.8 = (f32[128]{0:T(128)S(1)}, f32[128]{0:T(128)}, u32[]{:S(2)}) copy-start(f32[128]{0:T(128)} %param.22) | copy-start | bytes 1540
  218.0 43.4 %all-to-all-start = ((bf16[2,512,128]{2,0,1:T(2,128)(2,1)}), bf16[2,512,128]{2,0,1:T(2,128)(2,1)S(1)}, u32[]{:S(2)}, u32[]{:S(2)}) async-start(bf16[2,512,128]{2,0,1:T(2,128)(2,1)} %copy.58), calls=%async_computation | async-start | bytes 524288 | tf_op jit(solution)/shard_map/all_to_all | solution.py:136
  261.4 4.8 %copy-start.6 = (f32[128,2]{0,1:T(2,128)S(1)}, f32[128,2]{0,1:T(2,128)}, u32[]{:S(2)}) copy-start(f32[128,2]{0,1:T(2,128)} %param.28) | copy-start | bytes 3076
  261.4 52.8 %all-to-all-start.2 = ((bf16[128,4,2048]{2,1,0:T(4,128)(2,1)}), bf16[128,4,2048]{2,1,0:T(4,128)(2,1)S(1)}, u32[]{:S(2)}, u32[]{:S(2)}) async-start(bf16[128,4,2048]{2,1,0:T(4,128)(2,1)} %copy.66), calls=%async_computation.3 | async-start | bytes 4194304 | tf_op jit(solution)/shard_map/all_to_all | solution.py:154
Sparse Core Ops, SparseCore 0:
  126.6 39.6 all-gather.2
  168.4 38.9 all-gather.4
Sparse Core Ops, SparseCore 1:
  183.9 72.9 reduce-scatter.1
